TPU v7x, 32 devices: a whole 2x2x4 slice. The times are simulated.
32 devices in a mesh: sp: 4 (over z), dp: 8 (over y, x, core).
Axes of the slice: x: 2, y: 2, z: 4, core: 2. Of those that a mesh axis runs over, the one named last changes fastest.
Arguments:
- hidden: bfloat16 [8, 512, 2048], P('dp', 'sp'), may hold values from -6 to 6
- queries: bfloat16 [8, 512, 1024], P('dp', 'sp'), may hold values from -6 to 6
- values: bfloat16 [8, 512, 2048], P('dp', 'sp'), may hold values from -6 to 6
- key_weight: bfloat16 [2048, 1024], P('dp'), may hold values from -0.125 to 0.125
- decay_down: bfloat16 [2048, 16], replicated, may hold values from -0.125 to 0.125
- decay_up: float32 [16, 1024], replicated, may hold values from -1.5 to 1.5
- decay_bias: float32 [1024], replicated, may hold values from -1 to 8
- span_shift: bfloat16 [8, 512], P('dp', 'sp'), may hold values from -1.5 to 1.5, as said below
- norm_gain: float32 [2048], replicated, may hold values from 0.1 to 1.9
Outputs:
- attended: bfloat16 [8, 512, 2048], P('dp', 'sp')
Inputs may be any that keep to these rules, and one draw needn't show every extreme that they name: `span_shift`: constant over each aligned block of 64 positions.
All inputs are finite; a program needn't handle non-finite values.
Results may differ from a plain program's by a relative error of at most 0.0073.
Values may be sent and summed in bfloat16 or wider, within the bound.
A program may use at most 64 MiB of HBM per device.

v0:
```python
import jax
import jax.numpy as jnp
from jax import lax
from jax.sharding import PartitionSpec as P

HEADS = 4
DK = 256
DV = 512
BLOCK = 64
KEY = 1024
VAL = 2048


decay_tau = 16.0
norm_eps = 1e-05
highest = lax.Precision.HIGHEST


def mechanism(query, keys_in, value_in, log_decay):
    length, key_width = query.shape
    value_width = value_in.shape[-1]
    blocks = length // BLOCK
    step_decay = log_decay.reshape(blocks, BLOCK, key_width)
    inclusive = jnp.cumsum(step_decay, axis=1)
    exclusive = inclusive - step_decay
    total = inclusive[:, -1, :]
    query3 = query.reshape(blocks, BLOCK, key_width)
    keys3 = keys_in.reshape(blocks, BLOCK, key_width)
    value_tensor3 = value_in.reshape(blocks, BLOCK, value_width)
    query_forward_part = (query3 * jnp.exp(inclusive)).astype(jnp.bfloat16)
    key_fwd = (keys3 * jnp.exp(-inclusive)).astype(jnp.bfloat16)
    query_reverse_part = (query3 * jnp.exp(-exclusive)).astype(jnp.bfloat16)
    key_bwd = (keys3 * jnp.exp(exclusive)).astype(jnp.bfloat16)
    key_end = (keys3 * jnp.exp(total[:, None, :] - inclusive)).astype(jnp.bfloat16)
    fwd_scores = jnp.einsum(
        "nid,njd->nij", query_forward_part, key_fwd, preferred_element_type=jnp.float32
    )
    bwd_scores = jnp.einsum(
        "nid,njd->nij", query_reverse_part, key_bwd, preferred_element_type=jnp.float32
    )
    row_index = lax.broadcasted_iota(jnp.int32, (BLOCK, BLOCK), 0)
    col_index = lax.broadcasted_iota(jnp.int32, (BLOCK, BLOCK), 1)
    attention_scores = jnp.where((col_index <= row_index)[None], fwd_scores, bwd_scores).astype(
        jnp.bfloat16
    )
    inner_block_term = jnp.einsum(
        "ucy,uyh->uch", attention_scores, value_tensor3, preferred_element_type=jnp.float32
    )
    end_terms = jnp.einsum(
        "njd,nje->nde", key_end, value_tensor3, preferred_element_type=jnp.float32
    )
    start_terms = jnp.einsum(
        "njd,nje->nde", key_bwd, value_tensor3, preferred_element_type=jnp.float32
    )
    rates = jnp.exp(total)

    def forward_step(carry_state, inputs):
        rate, term = inputs
        return (rate[:, None] * carry_state + term, carry_state)

    def backward_step(carry_state, inputs):
        rate, term = inputs
        state_here = rate[:, None] * carry_state
        return (state_here + term, state_here)

    empty = jnp.zeros((key_width, value_width), jnp.float32)
    _, forward_scan_states = lax.scan(forward_step, empty, (rates, end_terms))
    _, reverse_scan_states = lax.scan(backward_step, empty, (rates, start_terms), reverse=True)
    produced_rows = jnp.einsum(
        "tzv,tvg->tzg",
        query_forward_part,
        forward_scan_states.astype(jnp.bfloat16),
        preferred_element_type=jnp.float32,
    )
    produced_rows = produced_rows + jnp.einsum(
        "tzv,tvg->tzg",
        query_reverse_part,
        reverse_scan_states.astype(jnp.bfloat16),
        preferred_element_type=jnp.float32,
    )
    return (inner_block_term + produced_rows).reshape(length, value_width).astype(jnp.bfloat16)


def body(
    hidden, queries, values, key_weight, decay_down, decay_up, decay_bias, span_shift, norm_gain
):
    seq_count, tok_count, model_width = hidden.shape
    group_size = lax.axis_size("sp")
    value_split = group_size // HEADS
    part_width = DV // value_split
    head_index = lax.axis_index("sp") // value_split
    token_rows = hidden.reshape(tok_count, model_width)

    def per_item(tensor, width):
        by_head = tensor.reshape(tok_count, HEADS, width).transpose(1, 0, 2)
        spread_out = jnp.broadcast_to(by_head[:, None], (HEADS, value_split, tok_count, width))
        return spread_out.reshape(group_size, tok_count, width)

    def every_item(tensor):
        return jnp.broadcast_to(tensor[None], (group_size,) + tensor.shape)

    key_sums = jnp.dot(
        token_rows,
        lax.all_gather(key_weight, "dp", axis=0, tiled=True),
        preferred_element_type=jnp.float32,
    )
    keys = key_sums.astype(jnp.bfloat16)
    head_key = lax.all_to_all(per_item(keys, DK), "sp", split_axis=0, concat_axis=1, tiled=True)[0]
    low = jnp.dot(token_rows, decay_down, preferred_element_type=jnp.float32).astype(jnp.bfloat16)
    value_items = values.reshape(tok_count, group_size, part_width).transpose(1, 0, 2)
    head_query, head_value, head_low, head_shift = (
        lax.all_to_all(
            per_item(queries.reshape(tok_count, KEY), DK),
            "sp",
            split_axis=0,
            concat_axis=1,
            tiled=True,
        ),
        lax.all_to_all(value_items, "sp", split_axis=0, concat_axis=1, tiled=True),
        lax.all_to_all(every_item(low), "sp", split_axis=0, concat_axis=1, tiled=True),
        lax.all_to_all(
            every_item(span_shift.reshape(tok_count, 1)),
            "sp",
            split_axis=0,
            concat_axis=1,
            tiled=True,
        ),
    )
    up_columns = lax.dynamic_slice_in_dim(decay_up, head_index * DK, DK, 1)
    bias_part = lax.dynamic_slice_in_dim(decay_bias, head_index * DK, DK, 0)
    pre = jnp.dot(
        head_low[0].astype(jnp.float32),
        up_columns,
        precision=highest,
        preferred_element_type=jnp.float32,
    )
    pre = pre + bias_part[None, :] + head_shift[0].astype(jnp.float32)
    log_decay = jax.nn.log_sigmoid(pre) / decay_tau
    scaled = head_query[0].astype(jnp.float32) * DK ** (-0.5)
    mixed = mechanism(scaled, head_key.astype(jnp.float32), head_value[0], log_decay)
    returned = lax.all_to_all(mixed[None], "sp", split_axis=1, concat_axis=0, tiled=True)
    grouped = returned.astype(jnp.float32).transpose(1, 0, 2).reshape(tok_count, HEADS, DV)
    normed = grouped * lax.rsqrt(jnp.mean(grouped * grouped, axis=-1, keepdims=True) + norm_eps)
    normed = normed * norm_gain.reshape(HEADS, DV)[None]
    return normed.reshape(seq_count, tok_count, VAL).astype(jnp.bfloat16)


def solution(mesh):
    in_specs = (
        P("dp", "sp", None),
        P("dp", "sp", None),
        P("dp", "sp", None),
        P("dp", None),
        P(),
        P(),
        P(),
        P("dp", "sp"),
        P(),
    )
    out_specs = P("dp", "sp", None)
    return jax.shard_map(body, mesh=mesh, in_specs=in_specs, out_specs=out_specs, check_vma=False)
```

profile of v0, /device:TPU:0, one launch (start us, length us, event | category | flops | bytes accessed | tf_op | source)
XLA Modules:
  0.0 159.2 jit_solution(2826352887242074970)
XLA Ops:
  7.3 1.2 broadcast_in_dim.46
  8.5 6.3 %all-to-all-start.2 = ((bf16[4,128,1]{1,2,0:T(2,128)(2,1)}), bf16[4,128,1]{1,2,0:T(2,128)(2,1)S(1)}, u32[]{:S(2)}, u32[]{:S(2)}) async-start(bf16[4,128,1]{1,2,0:T(2,128)(2,1)} %broadcast_in_dim.46), calls=%async_computation.2 | async-start | bytes 4096 | tf_op jit(solution)/shard_map/all_to_all | solution.py:121
  15.9 4.4 %all-to-all-done.2 = bf16[4,128,1]{1,2,0:T(2,128)(2,1)S(1)} async-done(((bf16[4,128,1]{1,2,0:T(2,128)(2,1)}), bf16[4,128,1]{1,2,0:T(2,128)(2,1)S(1)}, u32[]{:S(2)}, u32[]{:S(2)}) %all-to-all-start.2) | async-done | bytes 1056 | tf_op jit(solution)/shard_map/all_to_all | solution.py:121
  21.0 3.3 %all-to-all-start.1 = ((bf16[4,128,16]{1,2,0:T(8,128)(2,1)}), bf16[4,128,16]{1,2,0:T(8,128)(2,1)S(1)}, u32[]{:S(2)}, u32[]{:S(2)}) async-start(bf16[4,128,16]{1,2,0:T(8,128)(2,1)} %broadcast_in_dim.44), calls=%async_computation.1 | async-start | bytes 32768 | tf_op jit(solution)/shard_map/all_to_all | solution.py:120
  24.2 1.8 %copy.72 = bf16[1,128,1024]{1,2,0:T(8,128)(2,1)} copy(bf16[1,128,1024]{2,1,0:T(8,128)(2,1)} %param.14) | data formatting | bytes 524288 | tf_op args[1]
  26.0 3.8 %all-to-all-done.1 = bf16[4,128,16]{1,2,0:T(8,128)(2,1)S(1)} async-done(((bf16[4,128,16]{1,2,0:T(8,128)(2,1)}), bf16[4,128,16]{1,2,0:T(8,128)(2,1)S(1)}, u32[]{:S(2)}, u32[]{:S(2)}) %all-to-all-start.1) | async-done | bytes 16416 | tf_op jit(solution)/shard_map/all_to_all | solution.py:120
  29.8 3.4 %all-to-all-start = ((bf16[4,128,256]{1,2,0:T(8,128)(2,1)}), bf16[4,128,256]{1,2,0:T(8,128)(2,1)S(1)}, u32[]{:S(2)}, u32[]{:S(2)}) async-start(bf16[4,128,256]{1,2,0:T(8,128)(2,1)} %bitcast.1), calls=%async_computation | async-start | bytes 524288 | tf_op jit(solution)/shard_map/all_to_all | solution.py:112
  35.3 13.3 %all-gather.2.cloned.1.call-done = bf16[2048,1024]{1,0:T(8,128)(2,1)} async-done(((bf16[256,1024]{1,0:T(8,128)(2,1)}), bf16[2048,1024]{1,0:T(8,128)(2,1)}) %all-gather.2.cloned.1.call-update) | async-done | bytes 4194320 | tf_op jit(solution)/shard_map/all_gather | solution.py:104
  48.6 2.9 %convolution_convert_fusion = bf16[128,1024]{1,0:T(8,128)(2,1)S(1)} fusion(bf16[2048,1024]{1,0:T(8,128)(2,1)} %all-gather.2.cloned.1.call-done, bf16[1,128,2048]{2,1,0:T(8,128)(2,1)S(1)} %copy-done), kind=kOutput, calls=%fused_computation.18 | convolution fusion | flops 537001984 | bytes 4980736 | tf_op jit(solution)/shard_map/dot_general | solution.py:102
  52.2 4.6 %all-to-all-start.3 = ((bf16[4,128,256]{2,1,0:T(8,128)(2,1)}), bf16[4,128,256]{2,1,0:T(8,128)(2,1)S(1)}, u32[]{:S(2)}, u32[]{:S(2)}) async-start(bf16[4,128,256]{2,1,0:T(8,128)(2,1)} %bitcast.59), calls=%async_computation.3 | async-start | bytes 524288 | tf_op jit(solution)/shard_map/all_to_all | solution.py:108
  56.8 1.4 fusion.12
  59.3 6.8 %all-to-all-done.3 = bf16[4,128,256]{2,1,0:T(8,128)(2,1)S(1)} async-done(((bf16[4,128,256]{2,1,0:T(8,128)(2,1)}), bf16[4,128,256]{2,1,0:T(8,128)(2,1)S(1)}, u32[]{:S(2)}, u32[]{:S(2)}) %all-to-all-start.3) | async-done | bytes 262176 | tf_op jit(solution)/shard_map/all_to_all | solution.py:108
  66.8 3.7 %all-to-all-start.4 = ((bf16[4,128,512]{2,1,0:T(8,128)(2,1)}), bf16[4,128,512]{2,1,0:T(8,128)(2,1)S(1)}, u32[]{:S(2)}, u32[]{:S(2)}) async-start(bf16[4,128,512]{2,1,0:T(8,128)(2,1)} %bitcast.57), calls=%async_computation.4 | async-start | bytes 1048576 | tf_op jit(solution)/shard_map/all_to_all | solution.py:119
  72.6 3.1 %multiply_convert_fusion.4 = (bf16[8,64,256]{2,0,1:T(8,128)(2,1)}, bf16[8,64,256]{2,0,1:T(8,128)(2,1)S(1)}, bf16[8,64,256]{2,0,1:T(8,128)(2,1)S(1)}, bf16[8,64,256]{2,0,1:T(8,128)(2,1)S(1)}, bf16[8,64,256]{2,0,1:T(8,128)(2,1)}) fusion(f32[8,64,256]{2,0,1:T(8,128)S(1)} %fusion.15, f32[8,64,256]{2,1,0:T(8,128)S(1)} %convert.4, f32[8,64,256]{2,1,0:T(8,128)} %bitcast.82, ...), kind=kLoop, calls=%fused_computation.32 | loop fusion | flops 1835008 | bytes 3416064 | tf_op jit(solution)/shard_map/convert_element_type | solution.py:31
  75.7 7.6 %all-to-all-done.4 = bf16[4,128,512]{2,1,0:T(8,128)(2,1)S(1)} async-done(((bf16[4,128,512]{2,1,0:T(8,128)(2,1)}), bf16[4,128,512]{2,1,0:T(8,128)(2,1)S(1)}, u32[]{:S(2)}, u32[]{:S(2)}) %all-to-all-start.4) | async-done | bytes 524320 | tf_op jit(solution)/shard_map/all_to_all | solution.py:119
  83.3 2.7 %fusion.21 = f32[8,256,512]{2,1,0:T(8,128)} fusion(bf16[8,64,512]{2,1,0:T(8,128)(2,1)S(1)} %bitcast.75, bf16[8,64,256]{2,0,1:T(8,128)(2,1)S(1)} %get-tuple-element.194), kind=kOutput, calls=%fused_computation.43 | convolution fusion | flops 134217728 | bytes 4980736 | tf_op jit(solution)/shard_map/njd,nje->nde/dot_general | solution.py:52
  86.0 1.5 broadcast.22.clone
  87.6 16.1 %while.31 = (s32[]{:T(128)}, f32[256,512]{1,0:T(8,128)S(1)}, bf16[8,256,512]{2,1,0:T(8,128)(2,1)}, f32[8,256]{1,0:T(8,128)S(1)}, f32[8,256,512]{2,1,0:T(8,128)}, /*index=5*/s32[]{:T(128)}, s32[]{:T(128)}, s32[]{:T(128)}) while((s32[]{:T(128)}, f32[256,512]{1,0:T(8,128)S(1)}, bf16[8,256,512]{2,1,0:T(8,128)(2,1)}, ...), condition=%wide.region_4.5_spmd.clone, body=%wide.region_3.4_spmd.clone.sunk | while | flops 655364 | bytes 2625656 | solution.py:68
  88.4 1.2 bitcast_add_fusion.5
  90.4 1.2 bitcast_add_fusion.5
  92.4 1.2 bitcast_add_fusion.5
  94.5 1.2 bitcast_add_fusion.5
  96.5 1.2 bitcast_add_fusion.5
  103.7 2.7 %fusion.17 = f32[8,256,512]{2,1,0:T(8,128)} fusion(bf16[8,64,512]{2,1,0:T(8,128)(2,1)S(1)} %bitcast.76, bf16[8,64,256]{2,0,1:T(8,128)(2,1)S(1)} %copy-done.4), kind=kOutput, calls=%fused_computation.39 | convolution fusion | flops 134217728 | bytes 4980736 | tf_op jit(solution)/shard_map/njd,nje->nde/dot_general | solution.py:49
  106.4 1.5 broadcast.22.clone.1
  107.9 15.5 %while.30 = (s32[]{:T(128)}, f32[256,512]{1,0:T(8,128)S(1)}, bf16[8,256,512]{2,1,0:T(8,128)(2,1)}, f32[8,256]{1,0:T(8,128)S(1)}, f32[8,256,512]{2,1,0:T(8,128)}, /*index=5*/s32[]{:T(128)}, s32[]{:T(128)}) while((s32[]{:T(128)}, f32[256,512]{1,0:T(8,128)S(1)}, bf16[8,256,512]{2,1,0:T(8,128)(2,1)}, f32[8,256]{1,0:T(8,128)S(1)}, ...), condition=%wide.region_2.3_spmd.clone, body=%wide.region_1.2_spmd.clone.sunk | while | flops 524291 | bytes 2362976 | solution.py:67
  123.4 2.2 %fusion = f32[8,64,512]{2,1,0:T(8,128)S(1)} fusion(bf16[8,256,512]{2,1,0:T(8,128)(2,1)} %get-tuple-element.136, bf16[8,64,256]{2,0,1:T(8,128)(2,1)S(1)} %get-tuple-element.195), kind=kOutput, calls=%fused_computation.7 | convolution fusion | flops 134217728 | bytes 3407872 | tf_op jit(solution)/shard_map/tzv,tvg->tzg/dot_general | solution.py:75
  128.1 3.8 %reduce = bf16[512,512]{1,0:T(8,128)(2,1)S(1)} reduce(bf16[512,1,512]{2,1,0:T(2,128)(2,1)S(1)} %bitcast.78, bf16[]{:T(256)} %broadcast.39), dimensions={1}, to_apply=%bitcast.60.reduce_sub_computation | reduce | bytes 1048578
  131.9 1.2 reshape.113
  133.1 3.5 %all-to-all-start.5 = ((bf16[4,2,32768]{2,1,0:T(2,128)(2,1)}), bf16[4,2,32768]{2,1,0:T(2,128)(2,1)S(1)}, u32[]{:S(2)}, u32[]{:S(2)}) async-start(bf16[4,2,32768]{2,1,0:T(2,128)(2,1)} %reshape.113), calls=%async_computation.5 | async-start | bytes 1048576 | tf_op jit(solution)/shard_map/all_to_all | solution.py:141
  136.6 13.2 %all-to-all-done.5 = bf16[4,2,32768]{2,1,0:T(2,128)(2,1)S(1)} async-done(((bf16[4,2,32768]{2,1,0:T(2,128)(2,1)}), bf16[4,2,32768]{2,1,0:T(2,128)(2,1)S(1)}, u32[]{:S(2)}, u32[]{:S(2)}) %all-to-all-start.5) | async-done | bytes 524320 | tf_op jit(solution)/shard_map/all_to_all | solution.py:141
  151.2 1.2 convert_element_type.104
  (90 shorter events, 38.2 us)
Async XLA Ops:
  6.5 8.3 %copy-start = (bf16[1,128,2048]{2,1,0:T(8,128)(2,1)S(1)}, bf16[1,128,2048]{2,1,0:T(8,128)(2,1)}, u32[]{:S(2)}) copy-start(bf16[1,128,2048]{2,1,0:T(8,128)(2,1)} %param.13) | copy-start | bytes 1572868
  6.5 26.7 %copy-start.5 = (bf16[1,128,2048]{2,1,0:T(8,128)(2,1)S(1)}, bf16[1,128,2048]{2,1,0:T(8,128)(2,1)}, u32[]{:S(2)}) copy-start(bf16[1,128,2048]{2,1,0:T(8,128)(2,1)} %param.15) | copy-start | bytes 1572868
  6.5 42.0 %all-gather.2.cloned.1.call-start = ((), (), s32[]{:S(2)}) async-start(), calls=%async_computation.6 | async-start | bytes 4718592 | tf_op jit(solution)/shard_map/all_gather | solution.py:104
  8.5 11.8 %all-to-all-start.2 = ((bf16[4,128,1]{1,2,0:T(2,128)(2,1)}), bf16[4,128,1]{1,2,0:T(2,128)(2,1)S(1)}, u32[]{:S(2)}, u32[]{:S(2)}) async-start(bf16[4,128,1]{1,2,0:T(2,128)(2,1)} %broadcast_in_dim.46), calls=%async_computation.2 | async-start | bytes 4096 | tf_op jit(solution)/shard_map/all_to_all | solution.py:121
  21.0 8.8 %all-to-all-start.1 = ((bf16[4,128,16]{1,2,0:T(8,128)(2,1)}), bf16[4,128,16]{1,2,0:T(8,128)(2,1)S(1)}, u32[]{:S(2)}, u32[]{:S(2)}) async-start(bf16[4,128,16]{1,2,0:T(8,128)(2,1)} %broadcast_in_dim.44), calls=%async_computation.1 | async-start | bytes 32768 | tf_op jit(solution)/shard_map/all_to_all | solution.py:120
  29.8 22.4 %all-to-all-start = ((bf16[4,128,256]{1,2,0:T(8,128)(2,1)}), bf16[4,128,256]{1,2,0:T(8,128)(2,1)S(1)}, u32[]{:S(2)}, u32[]{:S(2)}) async-start(bf16[4,128,256]{1,2,0:T(8,128)(2,1)} %bitcast.1), calls=%async_computation | async-start | bytes 524288 | tf_op jit(solution)/shard_map/all_to_all | solution.py:112
  52.2 13.9 %all-to-all-start.3 = ((bf16[4,128,256]{2,1,0:T(8,128)(2,1)}), bf16[4,128,256]{2,1,0:T(8,128)(2,1)S(1)}, u32[]{:S(2)}, u32[]{:S(2)}) async-start(bf16[4,128,256]{2,1,0:T(8,128)(2,1)} %bitcast.59), calls=%async_computation.3 | async-start | bytes 524288 | tf_op jit(solution)/shard_map/all_to_all | solution.py:108
  58.2 0.8 copy-start.2
  66.1 0.7 copy-start.3
  66.8 16.5 %all-to-all-start.4 = ((bf16[4,128,512]{2,1,0:T(8,128)(2,1)}), bf16[4,128,512]{2,1,0:T(8,128)(2,1)S(1)}, u32[]{:S(2)}, u32[]{:S(2)}) async-start(bf16[4,128,512]{2,1,0:T(8,128)(2,1)} %bitcast.57), calls=%async_computation.4 | async-start | bytes 1048576 | tf_op jit(solution)/shard_map/all_to_all | solution.py:119
  87.6 16.1 %copy-start.4 = (bf16[8,64,256]{2,0,1:T(8,128)(2,1)S(1)}, bf16[8,64,256]{2,0,1:T(8,128)(2,1)}, u32[]{:S(2)}) copy-start(bf16[8,64,256]{2,0,1:T(8,128)(2,1)} %get-tuple-element.197) | copy-start | bytes 786436
  123.4 2.2 %copy-start.6 = (bf16[8,64,256]{2,0,1:T(8,128)(2,1)S(1)}, bf16[8,64,256]{2,0,1:T(8,128)(2,1)}, u32[]{:S(2)}) copy-start(bf16[8,64,256]{2,0,1:T(8,128)(2,1)} %get-tuple-element.193) | copy-start | bytes 786436
  123.4 2.4 %copy-start.1 = (bf16[8,256,512]{2,1,0:T(8,128)(2,1)S(1)}, bf16[8,256,512]{2,1,0:T(8,128)(2,1)}, u32[]{:S(2)}) copy-start(bf16[8,256,512]{2,1,0:T(8,128)(2,1)} %get-tuple-element.135) | copy-start | bytes 6291460
  127.5 9.0 %copy-start.7 = (f32[2048]{0:T(1024)S(1)}, f32[2048]{0:T(1024)}, u32[]{:S(2)}) copy-start(f32[2048]{0:T(1024)} %param.21) | copy-start | bytes 24580
  133.1 16.7 %all-to-all-start.5 = ((bf16[4,2,32768]{2,1,0:T(2,128)(2,1)}), bf16[4,2,32768]{2,1,0:T(2,128)(2,1)S(1)}, u32[]{:S(2)}, u32[]{:S(2)}) async-start(bf16[4,2,32768]{2,1,0:T(2,128)(2,1)} %reshape.113), calls=%async_computation.5 | async-start | bytes 1048576 | tf_op jit(solution)/shard_map/all_to_all | solution.py:141
Sparse Core Ops, SparseCore 0:
  9.2 39.2 all-gather.1
where the time goes:
time: 161 us; the launch traced here: 159 us
  waiting for transfers between devices  49.8 us (31%)
  other arithmetic  39.6 us (25%)
  starting transfers between devices  24.7 us (15%)
  local copies, waits for them, and re-layouts  16.8 us (10%)
  matrix products  14.1 us (9%)
  between operations  13.7 us (9%)
    all_gather x1, waiting for transfers between devices, body(): lax.all_gather(key_weight, 'dp', axis=0, tiled=True)  13.3 us
    all_to_all x1, waiting for transfers between devices, body(): lax.all_to_all(mixed[None], 'sp', split_axis=1, concat_axis=0, tiled=True)  13.2 us
    dynamic_update_slice x16, other arithmetic, mechanism(): _, forward_scan_states = lax.scan(forward_step, empty, (rates, end_terms))  12.6 us
    add x8, other arithmetic, backward_step(): return (state_here + term, state_here)  9.24 us
    add x8, other arithmetic, forward_step(): return (rate[:, None] * carry_state + term, carry_state)  9.24 us
    all_to_all x1, waiting for transfers between devices, body(): lax.all_to_all(value_items, 'sp', split_axis=0, concat_axis=1, tiled=True)  7.64 us
    all_to_all x1, waiting for transfers between devices, body(): lax.all_to_all(per_item(keys, DK), 'sp', split_axis=0, concat_axis=1, til...  6.78 us
    all_to_all x1, starting transfers between devices, body(): lax.all_to_all(every_item(span_shift.reshape(tok_count, 1)), 'sp', split_...  6.35 us
  transfers between devices with their start and end apart: 7, of which 6 were waited for; matrix products, arithmetic and copies ran while one was open for 11% of the time, Pallas kernels for 0%

commit v1 on v0

v1 whole, which is shorter than its diff:
```python
import functools

import jax
import jax.numpy as jnp
from jax import lax
from jax.experimental import pallas as pl
from jax.experimental.pallas import tpu as pltpu
from jax.sharding import PartitionSpec as P

HEADS = 4
DK = 256
DV = 512
BLOCK = 64
KEY = 1024
VAL = 2048
CORES = 2
SPLIT = 2
DVS = DV // SPLIT

decay_tau = 16.0
norm_eps = 1e-05
highest = lax.Precision.HIGHEST
MESH = pl.DeviceIdType.MESH
f32 = jnp.float32
bf16 = jnp.bfloat16


def each(low, high, fn):
    if high - low <= 4:
        for j in range(low, high):
            fn(j)
    else:
        lax.fori_loop(low, high, lambda j, c: (fn(j), c)[1], 0)


def dot_nt(a, b):
    return lax.dot_general(a, b, (((1,), (1,)), ((), ())), preferred_element_type=f32)


def dot_tn(a, b):
    return lax.dot_general(a, b, (((0,), (0,)), ((), ())), preferred_element_type=f32)


def kernel(
    n_sp, n_dp,
    hid, que, val, kw, down, up, bias, shift, gain,
    out,
    wbuf, hv, qv, vv, outv, qf, qb, qx, qs, fac, rate, local, sbuf, rbuf, acc,
    lsem, osem, wsend, wrecv, psend, precv, csend, crecv,
):
    sp = lax.axis_index("sp")
    dp = lax.axis_index("dp")
    chips = n_dp // CORES
    chip = dp // CORES
    core = dp % CORES
    partner = chip * CORES + (1 - core)
    tok = hv.shape[0]
    depth = kw.shape[0]

    def peer(j):
        return lax.rem(chip + j, chips) * CORES + core

    def source_chip(j):
        return lax.rem(chip - j + chips, chips)

    wlocal = [
        pltpu.make_async_copy(kw.at[:, pl.ds(h * DK, DK)], wbuf.at[h, dp], lsem.at[h])
        for h in range(HEADS)
    ]
    inputs = [
        pltpu.make_async_copy(a, b, lsem.at[HEADS + i])
        for i, (a, b) in enumerate(((hid, hv), (que, qv), (val, vv)))
    ]
    for c in wlocal + inputs:
        c.start()

    barrier = pltpu.get_barrier_semaphore()
    each(1, chips, lambda j: pl.semaphore_signal(
        barrier, inc=1, device_id={"dp": peer(j)}, device_id_type=MESH))
    pl.semaphore_signal(barrier, inc=1, device_id={"dp": partner}, device_id_type=MESH)

    for side in (1, n_sp - 1):
        pl.semaphore_signal(
            barrier, inc=1, device_id={"sp": lax.rem(sp + side, n_sp)}, device_id_type=MESH)
    pl.semaphore_wait(barrier, chips + 2)

    def wcopy(h, j):
        return pltpu.make_async_remote_copy(
            src_ref=wbuf.at[h, dp], dst_ref=wbuf.at[h, dp],
            send_sem=wsend.at[h, j], recv_sem=wrecv.at[h, j],
            device_id={"dp": peer(j)}, device_id_type=MESH)

    def wland(h, j):
        slot = wbuf.at[h, source_chip(j) * CORES + core]
        return pltpu.make_async_remote_copy(
            src_ref=slot, dst_ref=slot,
            send_sem=wsend.at[h, j], recv_sem=wrecv.at[h, j],
            device_id={"dp": peer(j)}, device_id_type=MESH)

    def pcopy(h, j):
        slot = wbuf.at[h, source_chip(j) * CORES + core]
        return pltpu.make_async_remote_copy(
            src_ref=slot, dst_ref=slot,
            send_sem=psend.at[h, j], recv_sem=precv.at[h, j],
            device_id={"dp": partner}, device_id_type=MESH)

    def pland(h, j):
        slot = wbuf.at[h, source_chip(j) * CORES + (1 - core)]
        return pltpu.make_async_remote_copy(
            src_ref=slot, dst_ref=slot,
            send_sem=psend.at[h, j], recv_sem=precv.at[h, j],
            device_id={"dp": partner}, device_id_type=MESH)

    for h in range(HEADS):
        wlocal[h].wait()
        each(1, chips, lambda j, h=h: wcopy(h, j).start())
        pcopy(h, 0).start()

    inputs[0].wait()
    low = dot_nt(hv[...], down[...]).astype(bf16)
    steps = shift[...].astype(f32)
    inputs[1].wait()
    row = lax.broadcasted_iota(jnp.int32, (tok, DK), 0)
    first = row < BLOCK
    ti = lax.broadcasted_iota(jnp.int32, (tok, tok), 0)
    tj = lax.broadcasted_iota(jnp.int32, (tok, tok), 1)
    same = (ti < BLOCK) == (tj < BLOCK)
    below = tj <= ti
    tri = jnp.where(same & below, 1.0, 0.0).astype(f32)
    for h in range(HEADS):
        cols = pl.ds(h * DK, DK)
        pre = jnp.dot(low.astype(f32), up[:, cols], precision=highest, preferred_element_type=f32)
        pre = pre + bias[:, cols] + jnp.where(first, steps[:, :1], steps[:, BLOCK:BLOCK + 1])
        logd = (jnp.minimum(pre, 0.0) - jnp.log1p(jnp.exp(-jnp.abs(pre)))) * (1.0 / decay_tau)
        incl = jnp.dot(tri, logd, precision=highest, preferred_element_type=f32)
        excl = incl - logd
        t0 = incl[BLOCK - 1:BLOCK, :]
        t1 = incl[tok - 1:tok, :]
        here = jnp.where(first, t0, t1)
        after = jnp.where(first, t1, 0.0)
        before = jnp.where(first, 0.0, t0)
        scaled = qv[:, cols].astype(f32) * DK ** (-0.5)
        qf[:, cols] = (scaled * jnp.exp(incl)).astype(bf16)
        qb[:, cols] = (scaled * jnp.exp(-excl)).astype(bf16)
        qx[:, cols] = (scaled * jnp.exp(here - excl)).astype(bf16)
        qs[0, :, cols] = (scaled * jnp.exp(incl + before)).astype(bf16)
        qs[1, :, cols] = (scaled * jnp.exp(here - excl + after)).astype(bf16)
        fac[0, :, cols] = jnp.exp(-incl)
        fac[1, :, cols] = jnp.exp(excl)
        fac[2, :, cols] = jnp.exp(here - incl)
        fac[3, :, cols] = jnp.exp(here - incl + after)
        fac[4, :, cols] = jnp.exp(excl + before)
        rate[:, cols] = jnp.exp(t0 + t1)
    inputs[2].wait()

    def chain(way, h, s):
        target = jnp.clip(sp + 1 - 2 * way, 0, n_sp - 1)
        return pltpu.make_async_remote_copy(
            src_ref=sbuf.at[way, h, s], dst_ref=rbuf.at[way, h, s],
            send_sem=csend.at[way, h, s], recv_sem=crecv.at[way, h, s],
            device_id={"sp": target}, device_id_type=MESH)

    def phase_keys(h):
        def relay(j):
            wland(h, j).wait_recv()
            pcopy(h, j).start()
        each(1, chips, relay)
        each(0, chips, lambda j: pland(h, j).wait_recv())
        cols = pl.ds(h * DK, DK)
        weights = wbuf[h].reshape(n_dp * depth, DK)
        keys = jnp.dot(hv[...], weights, preferred_element_type=f32).astype(bf16).astype(f32)
        v = vv[:, pl.ds(h * DV, DV)]
        k_fwd = (keys * fac[3, :, cols]).astype(bf16)
        k_bwd = (keys * fac[4, :, cols]).astype(bf16)
        for way, k in ((0, k_fwd), (1, k_bwd)):
            local[way, h] = dot_tn(v, k)

            @pl.when(sp == (0 if way == 0 else n_sp - 1))
            def _(way=way):
                for s in range(SPLIT):
                    sbuf[way, h, s] = local[way, h, pl.ds(s * DVS, DVS), :].astype(bf16)
                    chain(way, h, s).start()

        kf = (keys * fac[0, :, cols]).astype(bf16)
        kb = (keys * fac[1, :, cols]).astype(bf16)
        ke = (keys * fac[2, :, cols]).astype(bf16)
        query_f, query_b, query_x = qf[:, cols], qb[:, cols], qx[:, cols]
        lower = jnp.where(same, dot_nt(query_f, kf), dot_nt(query_f, ke))
        upper = jnp.where(same, dot_nt(query_b, kb), dot_nt(query_x, kb))
        scores = jnp.where(below, lower, upper).astype(bf16)
        acc[h] = jnp.dot(scores, v, preferred_element_type=f32)

    def phase_chain(way, h):
        cols = pl.ds(h * DK, DK)
        edge = way * (n_sp - 1)
        other = (1 - way) * (n_sp - 1)

        @pl.when(sp != edge)
        def _():
            for s in range(SPLIT):
                rows = pl.ds(s * DVS, DVS)
                chain(way, h, s).wait_recv()

                @pl.when(sp != other)
                def _(s=s, rows=rows):
                    state = rbuf[way, h, s].astype(f32) * rate[:, cols] + local[way, h, rows, :]
                    sbuf[way, h, s] = state.astype(bf16)
                    chain(way, h, s).start()

                acc[h, :, rows] += dot_nt(qs[way, :, cols], rbuf[way, h, s])

    def out_copy(h):
        cols = pl.ds(h * DV, DV)
        return pltpu.make_async_copy(outv.at[:, cols], out.at[:, cols], osem.at[h])

    def phase_out(h):
        cols = pl.ds(h * DV, DV)
        mixed = acc[h].astype(bf16).astype(f32)
        scale = lax.rsqrt(jnp.mean(mixed * mixed, axis=-1, keepdims=True) + norm_eps)
        outv[:, cols] = (mixed * scale * gain[:, cols]).astype(bf16)
        out_copy(h).start()

    near = jnp.where(sp * 2 < n_sp, 0, 1)
    far = 1 - near
    for step in range(HEADS + 2):
        if step < HEADS:
            phase_keys(step)
        if 0 <= step - 1 < HEADS:
            phase_chain(near, step - 1)
        if 0 <= step - 2 < HEADS:
            phase_chain(far, step - 2)
            phase_out(step - 2)

    for h in range(HEADS):
        each(1, chips, lambda j, h=h: wcopy(h, j).wait_send())
        each(0, chips, lambda j, h=h: pcopy(h, j).wait_send())
        for way in range(2):
            @pl.when(sp != (1 - way) * (n_sp - 1))
            def _(h=h, way=way):
                for s in range(SPLIT):
                    chain(way, h, s).wait_send()
        out_copy(h).wait()


def body(n_sp, n_dp, hidden, queries, values, key_weight, decay_down, decay_up, decay_bias,
         span_shift, norm_gain):
    seqs, length, width = hidden.shape
    tok = seqs * length
    assert tok == 2 * BLOCK
    chips = n_dp // CORES
    depth = key_weight.shape[0]
    anywhere = pl.BlockSpec(memory_space=pl.ANY)
    vmem = pl.BlockSpec(memory_space=pltpu.VMEM)
    dma = pltpu.SemaphoreType.DMA
    result = pl.pallas_call(
        functools.partial(kernel, n_sp, n_dp),
        out_shape=jax.ShapeDtypeStruct((tok, VAL), bf16),
        in_specs=[anywhere] * 4 + [vmem] * 5,
        out_specs=anywhere,
        scratch_shapes=[
            pltpu.VMEM((HEADS, n_dp, depth, DK), bf16),
            pltpu.VMEM((tok, width), bf16),
            pltpu.VMEM((tok, KEY), bf16),
            pltpu.VMEM((tok, VAL), bf16),
            pltpu.VMEM((tok, VAL), bf16),
            pltpu.VMEM((tok, KEY), bf16),
            pltpu.VMEM((tok, KEY), bf16),
            pltpu.VMEM((tok, KEY), bf16),
            pltpu.VMEM((2, tok, KEY), bf16),
            pltpu.VMEM((5, tok, KEY), f32),
            pltpu.VMEM((1, KEY), f32),
            pltpu.VMEM((2, HEADS, DV, DK), f32),
            pltpu.VMEM((2, HEADS, SPLIT, DVS, DK), bf16),
            pltpu.VMEM((2, HEADS, SPLIT, DVS, DK), bf16),
            pltpu.VMEM((HEADS, tok, DV), f32),
            dma((HEADS + 3,)),
            dma((HEADS,)),
            dma((HEADS, chips)),
            dma((HEADS, chips)),
            dma((HEADS, chips)),
            dma((HEADS, chips)),
            dma((2, HEADS, SPLIT)),
            dma((2, HEADS, SPLIT)),
        ],
        compiler_params=pltpu.CompilerParams(
            collective_id=0, has_side_effects=True, vmem_limit_bytes=62 * 1024 * 1024),
    )(
        hidden.reshape(tok, width), queries.reshape(tok, KEY), values.reshape(tok, VAL),
        key_weight, decay_down.T, decay_up, decay_bias.reshape(1, KEY),
        span_shift.reshape(1, tok), norm_gain.reshape(1, VAL),
    )
    return result.reshape(seqs, length, VAL)


def solution(mesh):
    in_specs = (
        P("dp", "sp", None), P("dp", "sp", None), P("dp", "sp", None), P("dp", None),
        P(), P(), P(), P("dp", "sp"), P(),
    )
    return jax.shard_map(
        functools.partial(body, mesh.shape["sp"], mesh.shape["dp"]),
        mesh=mesh, in_specs=in_specs, out_specs=P("dp", "sp", None), check_vma=False)
```

time: 161 us -> 65 us (0.40)
  Pallas kernels: 0 us -> 62.9 us
  waiting for transfers between devices: 49.8 us -> 0 us
  other arithmetic: 39.6 us -> 0 us
  starting transfers between devices: 24.7 us -> 0 us
  local copies, waits for them, and re-layouts: 16.8 us -> 1.88 us
  matrix products: 14.1 us -> 0 us
  between operations: 13.7 us -> 0.01 us
    pallas_call x0 -> x1, Pallas kernels: none -> 62.9 us  [body(): pl.pallas_call(functools.partial(kernel, n_sp, n_dp), out_shape=jax.Shape...]
    all_to_all x6 -> x0, waiting for transfers between devices: 35.9 us -> none  [the longest x1 13.2 us: body(): lax.all_to_all(mixed[None], 'sp', split_axis=1, concat_axis=0, tiled=True)]
    all_to_all x6 -> x0, starting transfers between devices: 24.7 us -> none  [the longest x1 6.35 us: body(): lax.all_to_all(every_item(span_shift.reshape(tok_count, 1)), 'sp', split_...]
    add x16 -> x0, other arithmetic: 18.5 us -> none  [the longest x8 9.24 us: backward_step(): return (state_here + term, state_here)]
    dot_general x9 -> x0, matrix products: 14.1 us -> none  [the longest x1 2.9 us: body(): jnp.dot(token_rows, lax.all_gather(key_weight, 'dp', axis=0, tiled=True),...]
    all_gather x1 -> x0, waiting for transfers between devices: 13.3 us -> none  [body(): lax.all_gather(key_weight, 'dp', axis=0, tiled=True)]
    dynamic_update_slice x16 -> x0, other arithmetic: 12.6 us -> none  [mechanism(): _, forward_scan_states = lax.scan(forward_step, empty, (rates, end_terms))]
    convert_element_type x4 -> x0, other arithmetic: 4.24 us -> none  [the longest x1 3.09 us: mechanism(): key_fwd = (keys3 * jnp.exp(-inclusive)).astype(jnp.bfloat16)]
  transfers between devices with their start and end apart: 7 -> 0, of which waited for: 6 -> 0; matrix products, arithmetic and copies ran while one was open for 11% -> 0% of each run, Pallas kernels for 0% -> 0%
where the time goes in v1:
time: 65 us; the launch traced here: 64.8 us
  Pallas kernels  62.9 us (97%)
  local copies, waits for them, and re-layouts  1.88 us (3%)
    pallas_call x1, Pallas kernels, body(): pl.pallas_call(functools.partial(kernel, n_sp, n_dp), out_shape=jax.Shape...  62.9 us
    unnamed x1, local copies, waits for them, and re-layouts  1.88 us

profile of v1, /device:TPU:0, one launch (start us, length us, event | category | flops | bytes accessed | tf_op | source)
XLA Modules:
  0.0 64.8 jit_solution(5248827406267036929)
XLA Ops:
  0.0 62.9 %shard_map.91 = bf16[128,2048]{1,0:T(8,128)(2,1)} custom-call(bf16[128,2048]{1,0:T(8,128)(2,1)} %bitcast.8, bf16[128,1024]{1,0:T(8,128)(2,1)} %bitcast.10, bf16[128,2048]{1,0:T(8,128)(2,1)} %bitcast.9, bf16[256,1024]{1,0:T(8,128)(2,1)} %kw.1, bf16[16,2048]{1,0:T(8,128)(2,1)} %bitcast.11, f32[16,1024]{1,0:T(8,128)} %up.1, f32[1,1024]{1,0:T(1,128)} %bitcast.13, ...), custom_call_target="tpu_custom_call" | custom-call | tf_op jit(solution)/shard_map/pallas_call | solution.py:255
  62.9 1.9 %copy.11 = bf16[1,128,2048]{2,1,0:T(8,128)(2,1)} copy(bf16[1,128,2048]{2,1,0:T(8,128)(2,1)} %bitcast.7) | data formatting | bytes 1048576

commit v2 on v1

--- a/solution.py
+++ b/solution.py
@@ -14,7 +14,7 @@
 KEY = 1024
 VAL = 2048
 CORES = 2
-SPLIT = 2
+SPLIT = 4
 DVS = DV // SPLIT
 
 decay_tau = 16.0
@@ -46,7 +46,7 @@
     hid, que, val, kw, down, up, bias, shift, gain,
     out,
     wbuf, hv, qv, vv, outv, qf, qb, qx, qs, fac, rate, local, sbuf, rbuf, acc,
-    lsem, osem, wsend, wrecv, psend, precv, csend, crecv,
+    lsem, osem, wsend, wrecv, psend, precv, csend, crecv, dsend, drecv,
 ):
     sp = lax.axis_index("sp")
     dp = lax.axis_index("dp")
@@ -57,10 +57,20 @@
     tok = hv.shape[0]
     depth = kw.shape[0]
 
+    square = chips == 4
+    half = depth // 2
+
+    def across(j):
+        return (chip + 1 - 2 * lax.rem(chip, 2), lax.rem(chip + 2, 4), 3 - chip)[j - 1]
+
     def peer(j):
+        if square:
+            return across(j) * CORES + core
         return lax.rem(chip + j, chips) * CORES + core
 
     def source_chip(j):
+        if square:
+            return chip if j == 0 else across(j)
         return lax.rem(chip - j + chips, chips)
 
     wlocal = [
@@ -111,10 +121,32 @@
             send_sem=psend.at[h, j], recv_sem=precv.at[h, j],
             device_id={"dp": partner}, device_id_type=MESH)
 
-    for h in range(HEADS):
+    direct = 3 if square else chips
+
+    def diagonal(h, i, lands):
+        origin = source_chip(3) if lands else source_chip(1 + i)
+        slot = wbuf.at[h, origin * CORES + core, pl.ds(i * half, half), :]
+        return pltpu.make_async_remote_copy(
+            src_ref=slot, dst_ref=slot,
+            send_sem=dsend.at[h, i], recv_sem=drecv.at[h, i],
+            device_id={"dp": peer(2 - i)}, device_id_type=MESH)
+
+    def phase_send(h):
         wlocal[h].wait()
-        each(1, chips, lambda j, h=h: wcopy(h, j).start())
+        each(1, direct, lambda j: wcopy(h, j).start())
         pcopy(h, 0).start()
+
+    def phase_relay(h):
+        def relay(j):
+            wland(h, j).wait_recv()
+            if square:
+                diagonal(h, j - 1, False).start()
+            pcopy(h, j).start()
+        each(1, direct, relay)
+
+    ahead = 2 if square else HEADS
+    for h in range(ahead):
+        phase_send(h)
 
     inputs[0].wait()
     low = dot_nt(hv[...], down[...]).astype(bf16)
@@ -127,7 +159,7 @@
     same = (ti < BLOCK) == (tj < BLOCK)
     below = tj <= ti
     tri = jnp.where(same & below, 1.0, 0.0).astype(f32)
-    for h in range(HEADS):
+    def phase_prep(h):
         cols = pl.ds(h * DK, DK)
         pre = jnp.dot(low.astype(f32), up[:, cols], precision=highest, preferred_element_type=f32)
         pre = pre + bias[:, cols] + jnp.where(first, steps[:, :1], steps[:, BLOCK:BLOCK + 1])
@@ -151,6 +183,7 @@
         fac[3, :, cols] = jnp.exp(here - incl + after)
         fac[4, :, cols] = jnp.exp(excl + before)
         rate[:, cols] = jnp.exp(t0 + t1)
+
     inputs[2].wait()
 
     def chain(way, h, s):
@@ -161,10 +194,10 @@
             device_id={"sp": target}, device_id_type=MESH)
 
     def phase_keys(h):
-        def relay(j):
-            wland(h, j).wait_recv()
-            pcopy(h, j).start()
-        each(1, chips, relay)
+        if square:
+            for i in range(2):
+                diagonal(h, i, True).wait_recv()
+            pcopy(h, 3).start()
         each(0, chips, lambda j: pland(h, j).wait_recv())
         cols = pl.ds(h * DK, DK)
         weights = wbuf[h].reshape(n_dp * depth, DK)
@@ -222,18 +255,29 @@
 
     near = jnp.where(sp * 2 < n_sp, 0, 1)
     far = 1 - near
-    for step in range(HEADS + 2):
-        if step < HEADS:
-            phase_keys(step)
-        if 0 <= step - 1 < HEADS:
-            phase_chain(near, step - 1)
-        if 0 <= step - 2 < HEADS:
-            phase_chain(far, step - 2)
-            phase_out(step - 2)
+    def relay_on(h):
+        if h < HEADS:
+            phase_relay(h)
+            if h + ahead < HEADS:
+                phase_send(h + ahead)
+
+    def phase_near(h):
+        phase_chain(near, h)
+
+    def phase_far(h):
+        phase_chain(far, h)
+        phase_out(h)
+
+    plan = ((phase_prep, 0), (relay_on, 0), (phase_prep, 1), (relay_on, 1), (phase_keys, 0), (phase_prep, 2), (relay_on, 2), (phase_keys, 1), (phase_prep, 3), (relay_on, 3), (phase_keys, 2), (phase_near, 0), (phase_keys, 3), (phase_near, 1), (phase_far, 0), (phase_near, 2), (phase_far, 1), (phase_near, 3), (phase_far, 2), (phase_far, 3))
+    for phase, h in plan:
+        phase(h)
 
     for h in range(HEADS):
-        each(1, chips, lambda j, h=h: wcopy(h, j).wait_send())
+        each(1, direct, lambda j, h=h: wcopy(h, j).wait_send())
         each(0, chips, lambda j, h=h: pcopy(h, j).wait_send())
+        if square:
+            for i in range(2):
+                diagonal(h, i, False).wait_send()
         for way in range(2):
             @pl.when(sp != (1 - way) * (n_sp - 1))
             def _(h=h, way=way):
@@ -281,6 +325,8 @@
             dma((HEADS, chips)),
             dma((2, HEADS, SPLIT)),
             dma((2, HEADS, SPLIT)),
+            dma((HEADS, 2)),
+            dma((HEADS, 2)),
         ],
         compiler_params=pltpu.CompilerParams(
             collective_id=0, has_side_effects=True, vmem_limit_bytes=62 * 1024 * 1024),

time: 65 us -> 59.7 us (0.918)
  Pallas kernels: 62.9 us -> 57.6 us
    pallas_call x1, Pallas kernels: 62.9 us -> 57.6 us  [body(): pl.pallas_call(functools.partial(kernel, n_sp, n_dp), out_shape=jax.Shape...]
where the time goes in v2:
time: 59.7 us; the launch traced here: 59.5 us
  Pallas kernels  57.6 us (96%)
  local copies, waits for them, and re-layouts  1.88 us (3%)
    pallas_call x1, Pallas kernels, body(): pl.pallas_call(functools.partial(kernel, n_sp, n_dp), out_shape=jax.Shape...  57.6 us
    unnamed x1, local copies, waits for them, and re-layouts  1.88 us

profile of v2, /device:TPU:0, one launch (start us, length us, event | category | flops | bytes accessed | tf_op | source)
XLA Modules:
  0.0 59.5 jit_solution(8158445587267491629)
XLA Ops:
  0.0 57.6 %shard_map.91 = bf16[128,2048]{1,0:T(8,128)(2,1)} custom-call(bf16[128,2048]{1,0:T(8,128)(2,1)} %bitcast.8, bf16[128,1024]{1,0:T(8,128)(2,1)} %bitcast.10, bf16[128,2048]{1,0:T(8,128)(2,1)} %bitcast.9, bf16[256,1024]{1,0:T(8,128)(2,1)} %kw.1, bf16[16,2048]{1,0:T(8,128)(2,1)} %bitcast.11, f32[16,1024]{1,0:T(8,128)} %up.1, f32[1,1024]{1,0:T(1,128)} %bitcast.13, ...), custom_call_target="tpu_custom_call" | custom-call | tf_op jit(solution)/shard_map/pallas_call | solution.py:299
  57.6 1.9 %copy.11 = bf16[1,128,2048]{2,1,0:T(8,128)(2,1)} copy(bf16[1,128,2048]{2,1,0:T(8,128)(2,1)} %bitcast.7) | data formatting | bytes 1048576
